TPU v7x, 32 devices: a whole 2x2x4 slice. The times are simulated.
32 devices in a mesh: fs: 8 (over z, x), tp: 4 (over y, core).
Axes of the slice: x: 2, y: 2, z: 4, core: 2. Of those that a mesh axis runs over, the one named last changes fastest.
Arguments:
- saved_input: bfloat16 [49152, 2048], P(('fs', 'tp')), may hold values from -6 to 6
- value_cotangent: bfloat16 [49152, 1024], P(('fs', 'tp')), may hold values from -0.0546875 to 0.0546875
- decay_cotangent: bfloat16 [49152, 16], P(('fs', 'tp')), may hold values from -0.02734375 to 0.02734375
- value_master: float32 [2048, 1024], P('fs', 'tp'), may hold values from -6 to 6
- value_factor: bfloat16 [2048, 256], P('fs'), may hold values from -0.22097087 to 0.22097087
- value_mean: float32 [256, 1024], P('fs', 'tp'), may hold values from -0.625 to 0.625
- value_second: float32 [256, 1024], P('fs', 'tp'), may hold values from 0.0001 to 0.1
- decay_master: float32 [2048, 16], replicated, may hold values from -6 to 6
- decay_mean: float32 [2048, 16], replicated, may hold values from -0.625 to 0.625
- decay_second: float32 [2048, 16], replicated, may hold values from 0.001 to 0.01
Outputs:
- value_step: float32 [2048, 1024], P('fs', 'tp')
- value_new: float32 [2048, 1024], P('fs', 'tp')
- value_copy: bfloat16 [2048, 1024], P(None, 'tp')
- mean_new: float32 [256, 1024], P('fs', 'tp')
- second_new: float32 [256, 1024], P('fs', 'tp')
- decay_step: float32 [2048, 16], replicated
- decay_copy: bfloat16 [2048, 16], replicated
All inputs are finite; a program needn't handle non-finite values.
Results may differ from a plain program's by a relative error of at most 0.0004.
Values may be sent and summed in bfloat16 or wider, within the bound.
No kernel may reach another device: no remote copies, remote signals or barrier semaphores. Data moves between devices by JAX's collectives and lax.ppermute only.
A program may use at most 64 MiB of HBM per device.

v0:
```python
import jax
import jax.numpy as jnp
from jax import lax
from jax.sharding import PartitionSpec as P

D = 2048
GW = 1024
BETA_ONE = 0.9
BETA_TWO = 0.99
ADAM_EPS = 1e-08
RMS_EPS = 1e-06
LEARN_RATE = 0.05
TOKEN_DIMS = (((0,), (0,)), ((), ()))


def adam_direction(moment_one, moment_two, gradient):
    mean_new = BETA_ONE * moment_one + (1.0 - BETA_ONE) * gradient
    second_new = BETA_TWO * moment_two + (1.0 - BETA_TWO) * gradient * gradient
    return (mean_new, second_new, mean_new / (jnp.sqrt(second_new) + ADAM_EPS))


def block_sum(left_parts, right_side):
    fs_count = lax.axis_size("fs")
    result = jnp.zeros(
        (lax.axis_size("fs") * (left_parts[0].shape[1] // fs_count), right_side.shape[1]),
        jnp.float32,
    )
    for left_side in left_parts:
        result = result + lax.dot_general(
            left_side, right_side, TOKEN_DIMS, preferred_element_type=jnp.float32
        )
    row_block = lax.psum_scatter(result, "fs", scatter_dimension=0, tiled=True)
    return lax.psum_scatter(row_block, "tp", scatter_dimension=1, tiled=True)


def local(
    saved_input,
    value_cotangent,
    decay_cotangent,
    value_master,
    value_factor,
    value_mean,
    value_second,
    decay_master,
    decay_mean,
    decay_second,
):
    decay_local = lax.dot_general(
        saved_input, decay_cotangent, TOKEN_DIMS, preferred_element_type=jnp.float32
    )
    decay_grad = lax.psum(decay_local, ("fs", "tp"))
    unused_mean, unused_second, decay_step = adam_direction(decay_mean, decay_second, decay_grad)
    decay_copy = (decay_master - LEARN_RATE * decay_step).astype(jnp.bfloat16)
    factor_wide = value_factor.astype(jnp.float32)
    mapped = jnp.dot(
        saved_input,
        lax.all_gather(value_factor, "fs", axis=0, tiled=True),
        preferred_element_type=jnp.float32,
    )
    high_part = lax.optimization_barrier(mapped.astype(jnp.bfloat16))
    low_part = (mapped - high_part.astype(jnp.float32)).astype(jnp.bfloat16)
    projected = block_sum((high_part, low_part), value_cotangent)
    mean_new, second_new, direction = adam_direction(value_mean, value_second, projected)
    raw_update = jnp.dot(
        factor_wide,
        lax.all_gather(direction, "fs", axis=0, tiled=True),
        precision=lax.Precision.HIGHEST,
        preferred_element_type=jnp.float32,
    )
    squares = lax.psum(jnp.sum(raw_update * raw_update), ("fs", "tp"))
    value_step = raw_update * lax.rsqrt(squares / (D * GW) + RMS_EPS)
    value_new = value_master - LEARN_RATE * value_step
    value_copy = lax.all_gather(value_new.astype(jnp.bfloat16), "fs", axis=0, tiled=True)
    return (value_step, value_new, value_copy, mean_new, second_new, decay_step, decay_copy)


def solution(mesh):
    in_specs = (
        P(("fs", "tp"), None),
        P(("fs", "tp"), None),
        P(("fs", "tp"), None),
        P("fs", "tp"),
        P("fs", None),
        P("fs", "tp"),
        P("fs", "tp"),
        P(),
        P(),
        P(),
    )
    out_specs = (
        P("fs", "tp"),
        P("fs", "tp"),
        P(None, "tp"),
        P("fs", "tp"),
        P("fs", "tp"),
        P(),
        P(),
    )
    return jax.shard_map(local, mesh=mesh, in_specs=in_specs, out_specs=out_specs, check_vma=False)
```

profile of v0, /device:TPU:0, one launch (start us, length us, event | category | flops | bytes accessed | tf_op | source)
XLA Modules:
  0.0 273.7 jit_solution(16057867461915626292)
XLA Ops:
  8.0 0.0 copy-start
  8.0 0.0 all-gather.3.cloned.1.call-start
  8.1 0.7 all-gather.3.cloned.1.call-update
  8.7 0.0 reduce-scatter.3.cloned.1.call-start
  8.8 45.2 %all-gather.3.cloned.1.call-done = bf16[2048,256]{1,0:T(8,128)(2,1)} async-done(((bf16[256,256]{1,0:T(8,128)(2,1)}), bf16[2048,256]{1,0:T(8,128)(2,1)}) %all-gather.3.cloned.1.call-update) | async-done | bytes 1048592 | tf_op jit(solution)/shard_map/all_gather | solution.py:57
  54.0 5.0 %fusion.8 = (bf16[1536,256]{1,0:T(8,128)(2,1)S(1)}, f32[1536,256]{1,0:T(8,128)S(1)}) fusion(bf16[1536,2048]{1,0:T(8,128)(2,1)} %param.10, bf16[2048,256]{1,0:T(8,128)(2,1)} %all-gather.3.cloned.1.call-done), kind=kOutput, calls=%fused_computation.16 | convolution fusion | flops 1611005952 | bytes 9699328 | tf_op jit(solution)/shard_map/dot_general | solution.py:55
  59.0 0.0 copy-done
  59.0 1.0 fusion.9
  60.0 0.0 copy-start.2
  60.0 2.0 convolution_add_fusion
  62.1 0.0 reduce-scatter.3.cloned.1.call-update
  62.1 0.0 reduce-scatter.5.cloned.1.call-start
  62.1 63.1 %reduce-scatter.3.cloned.1.call-done = f32[32,1024]{1,0:T(8,128)} async-done(((f32[256,1024]{1,0:T(8,128)}), f32[32,1024]{1,0:T(8,128)}) %reduce-scatter.3.cloned.1.call-update) | async-done | bytes 131088 | tf_op jit(solution)/shard_map/reduce_scatter | solution.py:32
  125.2 0.0 reduce-scatter.5.cloned.1.call-update
  125.2 0.0 copy-start.1
  125.2 0.0 all-reduce.2.cloned.1.call-start
  125.3 0.0 copy-done.2
  125.3 4.4 %fusion.10 = f32[2048,16]{0,1:T(8,128)} fusion(bf16[1536,16]{0,1:T(8,128)(2,1)S(1)} %copy-done.2, bf16[1536,2048]{1,0:T(8,128)(2,1)} %param.10), kind=kOutput, calls=%fused_computation.18 | convolution fusion | flops 100663296 | bytes 6471680 | tf_op jit(solution)/shard_map/dot_general | solution.py:48
  129.7 0.0 all-reduce.2.cloned.1.call-update
  129.7 0.0 all-gather.5.cloned.1.call-start
  129.8 1.1 copy.17
  130.8 15.4 %reduce-scatter.5.cloned.1.call-done = f32[32,256]{1,0:T(8,128)} async-done(((f32[32,1024]{1,0:T(8,128)}), f32[32,256]{1,0:T(8,128)}) %reduce-scatter.5.cloned.1.call-update) | async-done | bytes 32784 | tf_op jit(solution)/shard_map/reduce_scatter | solution.py:33
  146.3 1.4 add_divide_fusion
  147.7 30.8 %all_gather.10 = f32[256,256]{1,0:T(8,128)S(1)} all-gather(f32[32,256]{1,0:T(8,128)S(1)} %get-tuple-element.19), channel_id=1, replica_groups=mesh['fs'=8,'tp'=4] {'fs'}, dimensions={0}, use_global_device_ids=true | all-gather | bytes 294912 | tf_op jit(solution)/shard_map/all_gather | solution.py:66
  178.5 0.0 copy-done.1
  178.5 1.7 multiply_reduce_fusion
  180.2 38.8 %psum.14 = f32[]{:T(128)} all-reduce(f32[]{:T(128)} %get-tuple-element.24), channel_id=1, replica_groups=mesh['fs'=8,'tp'=4] {'fs','tp'}, use_global_device_ids=true, to_apply=%region_3.0 | all-reduce | flops 1 | bytes 8 | tf_op jit(solution)/shard_map/psum | solution.py:70
  219.7 1.8 fusion.6
  221.6 0.0 all-gather.5.cloned.1.call-update
  221.6 37.3 %all-reduce.2.cloned.1.call-done = f32[2048,16]{0,1:T(8,128)} async-done(((f32[2048,16]{0,1:T(8,128)}), f32[2048,16]{0,1:T(8,128)}) %all-reduce.2.cloned.1.call-update) | async-done | bytes 131088 | tf_op jit(solution)/shard_map/psum | solution.py:51
  258.9 1.9 subtract_convert_fusion.2
  260.7 1.8 copy.18
  262.5 1.8 copy.19
  264.3 0.0 all-gather.5.cloned.1.call-done
  264.3 2.3 copy.20
Async XLA Ops:
  8.0 51.0 %copy-start = (bf16[1536,1024]{1,0:T(8,128)(2,1)S(1)}, bf16[1536,1024]{1,0:T(8,128)(2,1)}, u32[]{:S(2)}) copy-start(bf16[1536,1024]{1,0:T(8,128)(2,1)} %param.11) | copy-start | bytes 9437188
  8.0 46.0 %all-gather.3.cloned.1.call-start = ((), (), s32[]{:S(2)}) async-start(), calls=%async_computation.2 | async-start | bytes 1179648 | tf_op jit(solution)/shard_map/all_gather | solution.py:57
  8.7 116.5 %reduce-scatter.3.cloned.1.call-start = ((), (), s32[]{:S(2)}) async-start(), calls=%async_computation.3 | async-start | bytes 1179648 | tf_op jit(solution)/shard_map/reduce_scatter | solution.py:32
  60.0 65.3 %copy-start.2 = (bf16[1536,16]{0,1:T(8,128)(2,1)S(1)}, bf16[1536,16]{0,1:T(8,128)(2,1)}, u32[]{:S(2)}) copy-start(bf16[1536,16]{0,1:T(8,128)(2,1)} %param.12) | copy-start | bytes 147460
  62.1 84.2 %reduce-scatter.5.cloned.1.call-start = ((), (), s32[]{:S(2)}) async-start(), calls=%async_computation.4 | async-start | bytes 163840 | tf_op jit(solution)/shard_map/reduce_scatter | solution.py:33
  125.2 53.3 %copy-start.1 = (bf16[256,256]{1,0:T(8,128)(2,1)S(1)}, bf16[256,256]{1,0:T(8,128)(2,1)}, u32[]{:S(2)}) copy-start(bf16[256,256]{1,0:T(8,128)(2,1)} %param.14) | copy-start | bytes 393220
  125.2 133.6 %all-reduce.2.cloned.1.call-start = ((), (), s32[]{:S(2)}) async-start(), calls=%async_computation.6 | async-start | bytes 262144 | tf_op jit(solution)/shard_map/psum | solution.py:51
  129.7 134.6 %all-gather.5.cloned.1.call-start = ((), (), s32[]{:S(2)}) async-start(), calls=%async_computation.5 | async-start | bytes 1179648 | tf_op jit(solution)/shard_map/all_gather | solution.py:73
Sparse Core Ops, SparseCore 0:
  10.9 42.9 all-gather.2
  62.2 62.9 reduce-scatter.2
  127.6 18.6 reduce-scatter.4
  221.7 41.0 all-gather.4
Sparse Core Ops, SparseCore 1:
  131.9 127.0 all-reduce.1
where the time goes:
time: 274 us
  waiting for transfers between devices  162 us (59%)
  blocking collectives  69.6 us (25%)
  between operations  16 us (6%)
  matrix products  14.1 us (5%)
  local copies, waits for them, and re-layouts  6.93 us (3%)
  other arithmetic  5.11 us (2%)
    reduce_scatter x1, waiting for transfers between devices, block_sum(): row_block = lax.psum_scatter(result, 'fs', scatter_dimension=0, tiled=True)  63.1 us
    all_gather x1, waiting for transfers between devices, local(): lax.all_gather(value_factor, 'fs', axis=0, tiled=True)  45.2 us
    psum x1, blocking collectives, local(): squares = lax.psum(jnp.sum(raw_update * raw_update), ('fs', 'tp'))  38.8 us
    psum x1, waiting for transfers between devices, local(): decay_grad = lax.psum(decay_local, ('fs', 'tp'))  37.3 us
    all_gather x1, blocking collectives, local(): lax.all_gather(direction, 'fs', axis=0, tiled=True)  30.8 us
    reduce_scatter x1, waiting for transfers between devices, block_sum(): return lax.psum_scatter(row_block, 'tp', scatter_dimension=1, tiled=True)  15.4 us
    unnamed x10, local copies, waits for them, and re-layouts  6.93 us
  transfers between devices with their start and end apart: 5, of which 4 were waited for; matrix products, arithmetic and copies ran while one was open for 6% of the time, Pallas kernels for 0%

commit v1 on v0

--- a/solution.py
+++ b/solution.py
@@ -11,6 +11,18 @@
 RMS_EPS = 1e-06
 LEARN_RATE = 0.05
 TOKEN_DIMS = (((0,), (0,)), ((), ()))
+
+
+def collect(shard, axis, dim):
+    ways, here = (lax.axis_size(axis), lax.axis_index(axis))
+    grown, reach = (shard, 1)
+    while reach < ways:
+        theirs = lax.ppermute(grown, axis, [(d, d ^ reach) for d in range(ways)])
+        mine_first = jnp.concatenate([grown, theirs], axis=dim)
+        theirs_first = jnp.concatenate([theirs, grown], axis=dim)
+        grown = jnp.where(here & reach == 0, mine_first, theirs_first)
+        reach = 2 * reach
+    return grown
 
 
 def adam_direction(moment_one, moment_two, gradient):
@@ -63,7 +75,7 @@
     mean_new, second_new, direction = adam_direction(value_mean, value_second, projected)
     raw_update = jnp.dot(
         factor_wide,
-        lax.all_gather(direction, "fs", axis=0, tiled=True),
+        collect(direction, "fs", 0),
         precision=lax.Precision.HIGHEST,
         preferred_element_type=jnp.float32,
     )

time: 274 us -> 305 us (1.11)
  waiting for transfers between devices: 162 us -> 216 us
  blocking collectives: 69.6 us -> 39.3 us
  starting transfers between devices: 0.2 us -> 5.58 us
    psum x1, waiting for transfers between devices: 37.3 us -> 80.6 us  [local(): decay_grad = lax.psum(decay_local, ('fs', 'tp'))]
    all_gather x1 -> x0, blocking collectives: 30.8 us -> none  [local(): lax.all_gather(direction, 'fs', axis=0, tiled=True)]
    reduce_scatter x1, waiting for transfers between devices: 15.4 us -> 21 us  [block_sum(): return lax.psum_scatter(row_block, 'tp', scatter_dimension=1, tiled=True)]
    ppermute x0 -> x3, starting transfers between devices: none -> 5.38 us  [collect(): theirs = lax.ppermute(grown, axis, [(d, d ^ reach) for d in range(ways)])]
    ppermute x0 -> x3, waiting for transfers between devices: none -> 5.26 us  [collect(): theirs = lax.ppermute(grown, axis, [(d, d ^ reach) for d in range(ways)])]
    unnamed x10 -> x14, local copies, waits for them, and re-layouts: 6.93 us -> 6.94 us
  transfers between devices with their start and end apart: 5 -> 8, of which waited for: 4 -> 6; matrix products, arithmetic and copies ran while one was open for 6% -> 5% of each run, Pallas kernels for 0% -> 0%
where the time goes in v1:
time: 305 us
  waiting for transfers between devices  216 us (71%)
  blocking collectives  39.3 us (13%)
  between operations  16 us (5%)
  matrix products  15.2 us (5%)
  local copies, waits for them, and re-layouts  6.94 us (2%)
  other arithmetic  5.75 us (2%)
  starting transfers between devices  5.58 us (2%)
    psum x1, waiting for transfers between devices, local(): decay_grad = lax.psum(decay_local, ('fs', 'tp'))  80.6 us
    reduce_scatter x1, waiting for transfers between devices, block_sum(): row_block = lax.psum_scatter(result, 'fs', scatter_dimension=0, tiled=True)  63.1 us
    all_gather x1, waiting for transfers between devices, local(): lax.all_gather(value_factor, 'fs', axis=0, tiled=True)  45.2 us
    psum x1, blocking collectives, local(): squares = lax.psum(jnp.sum(raw_update * raw_update), ('fs', 'tp'))  39.3 us
    reduce_scatter x1, waiting for transfers between devices, block_sum(): return lax.psum_scatter(row_block, 'tp', scatter_dimension=1, tiled=True)  21 us
    unnamed x14, local copies, waits for them, and re-layouts  6.94 us
  transfers between devices with their start and end apart: 8, of which 6 were waited for; matrix products, arithmetic and copies ran while one was open for 5% of the time, Pallas kernels for 0%

profile of v1, /device:TPU:0, one launch (start us, length us, event | category | flops | bytes accessed | tf_op | source)
XLA Modules:
  0.0 304.6 jit_solution(4708726695929272078)
XLA Ops:
  8.0 0.0 copy-start
  8.0 0.0 all-gather.3.cloned.1.call-start
  8.1 0.7 all-gather.3.cloned.1.call-update
  8.7 0.0 reduce-scatter.3.cloned.1.call-start
  8.8 45.2 %all-gather.3.cloned.1.call-done = bf16[2048,256]{1,0:T(8,128)(2,1)} async-done(((bf16[256,256]{1,0:T(8,128)(2,1)}), bf16[2048,256]{1,0:T(8,128)(2,1)}) %all-gather.3.cloned.1.call-update) | async-done | bytes 1048592 | tf_op jit(solution)/shard_map/all_gather | solution.py:69
  54.0 5.0 %fusion.16 = (bf16[1536,256]{1,0:T(8,128)(2,1)S(1)}, f32[1536,256]{1,0:T(8,128)S(1)}) fusion(bf16[1536,2048]{1,0:T(8,128)(2,1)} %param.10, bf16[2048,256]{1,0:T(8,128)(2,1)} %all-gather.3.cloned.1.call-done), kind=kOutput, calls=%fused_computation.27 | convolution fusion | flops 1611005952 | bytes 9699328 | tf_op jit(solution)/shard_map/dot_general | solution.py:67
  59.0 0.0 copy-done
  59.0 1.0 fusion.17
  60.0 0.0 copy-start.3
  60.0 0.0 copy-start.4
  60.0 0.0 copy-start.2
  60.0 2.0 convolution_add_fusion
  62.1 0.0 reduce-scatter.3.cloned.1.call-update
  62.1 0.0 reduce-scatter.5.cloned.1.call-start
  62.1 63.1 %reduce-scatter.3.cloned.1.call-done = f32[32,1024]{1,0:T(8,128)} async-done(((f32[256,1024]{1,0:T(8,128)}), f32[32,1024]{1,0:T(8,128)}) %reduce-scatter.3.cloned.1.call-update) | async-done | bytes 131088 | tf_op jit(solution)/shard_map/reduce_scatter | solution.py:44
  125.2 0.0 reduce-scatter.5.cloned.1.call-update
  125.3 0.0 all-reduce.2.cloned.1.call-start
  125.3 21.0 %reduce-scatter.5.cloned.1.call-done = f32[32,256]{1,0:T(8,128)} async-done(((f32[32,1024]{1,0:T(8,128)}), f32[32,256]{1,0:T(8,128)}) %reduce-scatter.5.cloned.1.call-update) | async-done | bytes 32784 | tf_op jit(solution)/shard_map/reduce_scatter | solution.py:45
  146.3 0.0 copy-done.3
  146.3 0.0 copy-done.4
  146.3 1.4 add_divide_fusion
  147.7 1.5 collective-permute-start
  149.2 2.5 collective-permute-done
  151.6 1.5 collective-permute-start.1
  153.2 2.8 collective-permute-done.1
  156.0 0.7 maximum_select_fusion.2
  156.6 0.0 copy-start.1
  156.6 2.4 collective-permute-start.2
  159.0 0.0 copy-done.2
  159.0 4.4 %fusion.18 = f32[2048,16]{0,1:T(8,128)} fusion(bf16[1536,16]{0,1:T(8,128)(2,1)S(1)} %copy-done.2, bf16[1536,2048]{1,0:T(8,128)(2,1)} %param.10), kind=kOutput, calls=%fused_computation.29 | convolution fusion | flops 100663296 | bytes 6471680 | tf_op jit(solution)/shard_map/dot_general | solution.py:60
  163.4 0.0 all-reduce.2.cloned.1.call-update
  163.4 0.0 all-gather.5.cloned.1.call-start
  163.5 1.1 copy.17
  164.6 0.0 collective-permute-done.2
  164.6 0.0 copy-done.1
  164.6 2.8 multiply_reduce_fusion
  167.4 39.3 %psum.14 = f32[]{:T(128)} all-reduce(f32[]{:T(128)} %get-tuple-element.24), channel_id=1, replica_groups=mesh['fs'=8,'tp'=4] {'fs','tp'}, use_global_device_ids=true, to_apply=%region_3.4 | all-reduce | flops 1 | bytes 8 | tf_op jit(solution)/shard_map/psum | solution.py:82
  207.4 1.8 fusion.14
  209.2 0.0 all-gather.5.cloned.1.call-update
  209.3 80.6 %all-reduce.2.cloned.1.call-done = f32[2048,16]{0,1:T(8,128)} async-done(((f32[2048,16]{0,1:T(8,128)}), f32[2048,16]{0,1:T(8,128)}) %all-reduce.2.cloned.1.call-update) | async-done | bytes 131088 | tf_op jit(solution)/shard_map/psum | solution.py:63
  289.8 1.9 subtract_convert_fusion.2
  291.7 1.8 copy.18
  293.5 1.8 copy.19
  295.2 0.0 all-gather.5.cloned.1.call-done
  295.3 2.3 copy.20
  (1 shorter events, 0.0 us)
Async XLA Ops:
  8.0 51.0 %copy-start = (bf16[1536,1024]{1,0:T(8,128)(2,1)S(1)}, bf16[1536,1024]{1,0:T(8,128)(2,1)}, u32[]{:S(2)}) copy-start(bf16[1536,1024]{1,0:T(8,128)(2,1)} %param.11) | copy-start | bytes 9437188
  8.0 46.0 %all-gather.3.cloned.1.call-start = ((), (), s32[]{:S(2)}) async-start(), calls=%async_computation.2 | async-start | bytes 1179648 | tf_op jit(solution)/shard_map/all_gather | solution.py:69
  8.7 116.5 %reduce-scatter.3.cloned.1.call-start = ((), (), s32[]{:S(2)}) async-start(), calls=%async_computation.3 | async-start | bytes 1179648 | tf_op jit(solution)/shard_map/reduce_scatter | solution.py:44
  60.0 86.3 %copy-start.3 = (f32[32,256]{1,0:T(8,128)S(1)}, f32[32,256]{1,0:T(8,128)}, u32[]{:S(2)}) copy-start(f32[32,256]{1,0:T(8,128)} %param.16) | copy-start | bytes 98308
  60.0 86.3 %copy-start.4 = (f32[32,256]{1,0:T(8,128)S(1)}, f32[32,256]{1,0:T(8,128)}, u32[]{:S(2)}) copy-start(f32[32,256]{1,0:T(8,128)} %param.15) | copy-start | bytes 98308
  60.0 99.0 %copy-start.2 = (bf16[1536,16]{0,1:T(8,128)(2,1)S(1)}, bf16[1536,16]{0,1:T(8,128)(2,1)}, u32[]{:S(2)}) copy-start(bf16[1536,16]{0,1:T(8,128)(2,1)} %param.12) | copy-start | bytes 147460
  62.1 84.2 %reduce-scatter.5.cloned.1.call-start = ((), (), s32[]{:S(2)}) async-start(), calls=%async_computation.4 | async-start | bytes 163840 | tf_op jit(solution)/shard_map/reduce_scatter | solution.py:45
  125.3 164.6 %all-reduce.2.cloned.1.call-start = ((), (), s32[]{:S(2)}) async-start(), calls=%async_computation.6 | async-start | bytes 262144 | tf_op jit(solution)/shard_map/psum | solution.py:63
  147.7 3.9 %collective-permute-start = (f32[32,256]{1,0:T(8,128)S(1)}, f32[32,256]{1,0:T(8,128)S(1)}, u32[]{:S(2)}, u32[]{:S(2)}) collective-permute-start(f32[32,256]{1,0:T(8,128)S(1)} %get-tuple-element.19), channel_id=1, source_target_pairs={{0,4},{4,0},{8,12},{12,8},{16,20},{20,16},{24,28},{28,24},{1,5},{5... | collective-permute-start | bytes 98312 | tf_op jit(solution)/shard_map/ppermute | solution.py:20
  151.6 4.3 %collective-permute-start.1 = (f32[64,256]{1,0:T(8,128)S(1)}, f32[64,256]{1,0:T(8,128)S(1)}, u32[]{:S(2)}, u32[]{:S(2)}) collective-permute-start(f32[64,256]{1,0:T(8,128)S(1)} %maximum_select_fusion.3), channel_id=1, source_target_pairs={{0,8},{4,12},{8,0},{12,4},{16,24},{20,28},{24,16},{28,20},{1,9},{5... | collective-permute-start | bytes 196616 | tf_op jit(solution)/shard_map/ppermute | solution.py:20
  156.6 7.9 %copy-start.1 = (bf16[256,256]{1,0:T(8,128)(2,1)S(1)}, bf16[256,256]{1,0:T(8,128)(2,1)}, u32[]{:S(2)}) copy-start(bf16[256,256]{1,0:T(8,128)(2,1)} %param.14) | copy-start | bytes 393220
  156.6 7.9 %collective-permute-start.2 = (f32[128,256]{1,0:T(8,128)}, f32[128,256]{1,0:T(8,128)}, u32[]{:S(2)}, u32[]{:S(2)}) collective-permute-start(f32[128,256]{1,0:T(8,128)} %maximum_select_fusion.2), channel_id=1, source_target_pairs={{0,16},{4,20},{8,24},{12,28},{16,0},{20,4},{24,8},{28,12},{1,17},{... | collective-permute-start | bytes 393224 | tf_op jit(solution)/shard_map/ppermute | solution.py:20
  163.4 131.8 %all-gather.5.cloned.1.call-start = ((), (), s32[]{:S(2)}) async-start(), calls=%async_computation.5 | async-start | bytes 1179648 | tf_op jit(solution)/shard_map/all_gather | solution.py:85
Sparse Core Ops, SparseCore 0:
  10.9 42.9 all-gather.2
  62.2 62.9 reduce-scatter.2
  127.7 18.5 reduce-scatter.4
  209.4 40.0 all-gather.4
Sparse Core Ops, SparseCore 1:
  163.5 126.2 all-reduce.1
